TPU v7x, 32 devices: a whole 2x2x4 slice. The times are simulated.
32 devices in a mesh: sp: 8 (over z, y), tp: 4 (over x, core).
Axes of the slice: x: 2, y: 2, z: 4, core: 2. Of those that a mesh axis runs over, the one named last changes fastest.
Arguments:
- stream: bfloat16 [8192, 4096], P('sp', 'tp'), may hold values from -11 to 11
- norm_gain: bfloat16 [3, 4096], P(None, 'tp'), may hold values from 0.099609375 to 1.8984375
- pool_weight: bfloat16 [3, 4, 1024, 1024], P(None, 'tp', 'sp'), may hold values from -0.1875 to 0.1875
- pool_scale: bfloat16 [3, 4096], P(None, 'tp'), may hold values from 0.099609375 to 1.8984375
Outputs:
- mixed: bfloat16 [8192, 4096], P('sp', 'tp')
All inputs are finite; a program needn't handle non-finite values.
Results may differ from a plain program's by a relative error of at most 0.015.
Values may be sent and summed in bfloat16 or wider, within the bound.
A program may use at most 64 MiB of HBM per device.

v0:
```python
import jax
import jax.numpy as jnp
from jax import lax
from jax.sharding import PartitionSpec as P

D = 4096
POOL_GROUPS = 4


norm_eps = 1e-06


def padded(value, sides, width):
    for axis, dim in sides:
        devices, length = (lax.axis_size(axis), value.shape[dim])
        up = [(i, (i + 1) % devices) for i in range(devices - 1)]
        down = [(j, i) for i, j in up]
        last = lax.slice_in_dim(value, length - width, length, axis=dim)
        initial = lax.slice_in_dim(value, 0, width, axis=dim)
        before = lax.ppermute(last, axis, up)
        after = lax.ppermute(initial, axis, down)
        value = jnp.concatenate([before, value, after], axis=dim)
    return value


def window_pool(extended, out_rows, centre, halves, seq_total, reach_rows, per_dev, group_width):
    ext_float = extended.astype(jnp.float32).reshape(extended.shape[0], per_dev, group_width)
    window_sums = jnp.zeros((out_rows, per_dev, group_width), jnp.float32)
    for offset in range(-reach_rows, reach_rows):
        in_window = ((offset >= -halves) & (offset < halves)).astype(jnp.float32)
        window_sums = (
            window_sums
            + ext_float[reach_rows + offset : reach_rows + offset + out_rows]
            * in_window[None, :, None]
        )
    low_end = jnp.maximum(centre[:, None] - halves[None, :], 0)
    high_end = jnp.minimum(centre[:, None] + halves[None, :], seq_total)
    counts = jnp.maximum(high_end - low_end, 1).astype(jnp.float32)
    middle = ext_float[reach_rows : reach_rows + out_rows]
    return (window_sums / counts[:, :, None] - middle).astype(jnp.bfloat16)


def local(stream, norm_gain, pool_weight, pool_scale):
    tok_rows, local_width = stream.shape
    layers, per_dev, shard_rows, group_width = pool_weight.shape
    reach_rows = 2**POOL_GROUPS // 2
    seq_total = tok_rows * lax.axis_size("sp")
    first_pos = lax.axis_index("sp") * tok_rows
    groups = lax.axis_index("tp") * per_dev + jnp.arange(per_dev, dtype=jnp.int32)
    halves = jnp.left_shift(jnp.int32(1), groups)
    deep_rows = reach_rows * layers
    current = padded(stream, (("sp", 0),), deep_rows)
    base_pos = first_pos - deep_rows
    for layer_idx in range(layers):
        ext_rows = current.shape[0]
        positions = base_pos + jnp.arange(ext_rows, dtype=jnp.int32)
        inside = (positions >= 0) & (positions < seq_total)
        current_f = current.astype(jnp.float32)
        square_sums = lax.psum(jnp.sum(current_f * current_f, axis=1), "tp")
        row_scale = lax.rsqrt(square_sums / D + norm_eps)
        normed = current_f * row_scale[:, None] * norm_gain[layer_idx].astype(jnp.float32)
        normed = jnp.where(inside[:, None], normed, 0.0).astype(jnp.bfloat16)
        out_rows = ext_rows - 2 * reach_rows
        residual = current_f[reach_rows : ext_rows - reach_rows]
        centre = positions[reach_rows : ext_rows - reach_rows]
        base_pos = base_pos + reach_rows
        pooled = window_pool(
            normed, out_rows, centre, halves, seq_total, reach_rows, per_dev, group_width
        )
        branch = jnp.einsum(
            "tgc,gcd->tgd",
            pooled,
            lax.all_gather(pool_weight[layer_idx], "sp", axis=1, tiled=True),
            preferred_element_type=jnp.float32,
        )
        branch = branch.reshape(out_rows, local_width)
        current = (residual + branch * pool_scale[layer_idx].astype(jnp.float32)).astype(
            jnp.bfloat16
        )
    return current


def solution(mesh):
    placed = (P("sp", "tp"), P(None, "tp"), P(None, "tp", "sp", None), P(None, "tp"))
    return jax.shard_map(
        local, mesh=mesh, in_specs=placed, out_specs=P("sp", "tp"), check_vma=False
    )
```

profile of v0, /device:TPU:0, one launch (start us, length us, event | category | flops | bytes accessed | tf_op | source)
XLA Modules:
  0.0 213.5 jit_solution(14513719529926578591)
XLA Ops:
  6.5 0.0 copy-start
  6.5 0.0 all-gather.7.cloned.1.call-start
  6.5 2.2 %fusion.70 = (bf16[1,1,128,1024]{3,2,1,0:T(8,128)(2,1)}, bf16[1,1,128,1024]{3,2,1,0:T(8,128)(2,1)}, bf16[1,1,128,1024]{3,2,1,0:T(8,128)(2,1)}) fusion(bf16[3,1,128,1024]{3,2,1,0:T(8,128)(2,1)} %param.6), kind=kLoop, calls=%fused_computation.141 | loop fusion | bytes 1572864 | tf_op jit(solution)/shard_map/slice | solution.py:73
  8.7 0.0 all-gather.7.cloned.1.call-update
  8.7 0.0 all-gather.9.cloned.1.call-start
  8.8 0.7 all-gather.9.cloned.1.call-update
  9.5 0.0 all-gather.11.cloned.1.call-start
  9.5 0.8 fusion.69
  10.4 4.9 %collective-permute-start = (bf16[24,1024]{1,0:T(8,128)(2,1)S(1)}, bf16[24,1024]{1,0:T(8,128)(2,1)S(1)}, u32[]{:S(2)}, u32[]{:S(2)}) collective-permute-start(bf16[24,1024]{1,0:T(8,128)(2,1)S(1)} %get-tuple-element.5), channel_id=1, source_target_pairs={{0,4},{4,8},{8,12},{12,16},{16,20},{20,24},{24,28},{1,5},{5,9},{9,... | collective-permute-start | bytes 147464 | tf_op jit(solution)/shard_map/ppermute | solution.py:20
  15.3 1.3 collective-permute-start.1
  16.6 0.0 all-gather.11.cloned.1.call-update
  16.6 0.8 slice_convert_fusion.1
  17.5 0.8 slice_convert_fusion
  18.3 0.1 maximum_convert_fusion.2
  18.4 0.1 maximum_convert_fusion.1
  18.5 0.1 maximum_convert_fusion.3
  18.7 0.0 collective-permute-done
  18.7 2.5 %collective-permute-done.1 = bf16[24,1024]{1,0:T(8,128)(2,1)S(1)} collective-permute-done((bf16[24,1024]{1,0:T(8,128)(2,1)S(1)}, bf16[24,1024]{1,0:T(8,128)(2,1)S(1)}, u32[]{:S(2)}, u32[]{:S(2)}) %collective-permute-start.1) | collective-permute-done | bytes 49184 | tf_op jit(solution)/shard_map/ppermute | solution.py:21
  21.2 0.0 copy-done
  21.2 0.5 multiply_reduce_fusion
  21.8 6.2 %psum.21 = f32[1072]{0:T(1024)S(1)} all-reduce(f32[1072]{0:T(1024)S(1)} %multiply_reduce_fusion), channel_id=1, replica_groups=mesh['sp'=8,'tp'=4] {'tp'}, use_global_device_ids=true, to_apply=%region_1.0 | all-reduce | flops 1072 | bytes 8576 | tf_op jit(solution)/shard_map/psum | solution.py:59
  27.9 2.5 %maximum_convert_fusion = f32[1072,1024]{1,0:T(8,128)} fusion(bf16[24,1024]{1,0:T(8,128)(2,1)S(1)} %collective-permute-done.1, bf16[1024,1024]{1,0:T(8,128)(2,1)S(1)} %copy-done, bf16[24,1024]{1,0:T(8,128)(2,1)S(1)} %collective-permute-done), kind=kLoop, calls=%fused_computation.115 | loop fusion | flops 6586368 | bytes 6586368 | tf_op jit(solution)/shard_map/convert_element_type | solution.py:58
  30.5 2.9 %fusion.59 = f32[1072,1024]{1,0:T(8,128)} fusion(f32[1024]{0:T(1024)S(1)} %bitcast.21, f32[1072]{0:T(1024)S(1)} %add_rsqrt_fusion.2, pred[1072]{0:T(1024)(128)(4,1)S(1)} %compare_and_fusion.2, bf16[24,1024]{1,0:T(8,128)(2,1)S(1)} %collective-permute-done.1, bf16[1024,1024]{1,0:T(8,128)(2,1)S(1)} %copy-done, bf16[24,1024]{1,0:T(8,128)(2,1)S(1)} %collective-permute-done), kind=kLoop, calls=%fused_computation.114 | loop fusion | flops 12075008 | bytes 6595824 | tf_op jit(solution)/shard_map/convert_element_type | solution.py:27
  33.4 28.0 %all-gather.7.cloned.1.call-done = bf16[1,1,1024,1024]{3,2,1,0:T(8,128)(2,1)} async-done(((bf16[1,1,128,1024]{3,2,1,0:T(8,128)(2,1)}), bf16[1,1,1024,1024]{3,2,1,0:T(8,128)(2,1)}) %all-gather.7.cloned.1.call-update) | async-done | bytes 2097168 | tf_op jit(solution)/shard_map/all_gather | solution.py:73
  61.4 42.3 %multiply_reduce_fusion.1 = (f32[1056]{0:T(1024)S(1)}, f32[1056,1024]{1,0:T(8,128)}) fusion(f32[1024]{0:T(1024)S(1)} %bitcast.24, bf16[1,1,1024,1024]{3,2,1,0:T(8,128)(2,1)} %all-gather.7.cloned.1.call-done, f32[1072,1024]{1,0:T(8,128)} %fusion.59, f32[1056]{0:T(1024)S(1)} %maximum_convert_fusion.2, f32[]{:T(128)S(6)} %mul.631, f32[]{:T(128)S(6)} %mul.628, ...), kind=kOutput, calls=%fused_computation.40 | convolution fusion | flops 2257845248 | bytes 79966528 | tf_op jit(solution)/shard_map/tgc,gcd->tgd/dot_general | solution.py:70
  103.7 6.3 %psum.22 = f32[1056]{0:T(1024)S(1)} all-reduce(f32[1056]{0:T(1024)S(1)} %get-tuple-element.16), channel_id=1, replica_groups=mesh['sp'=8,'tp'=4] {'tp'}, use_global_device_ids=true, to_apply=%region_3.4 | all-reduce | flops 1056 | bytes 8448 | tf_op jit(solution)/shard_map/psum | solution.py:59
  110.0 4.7 %fusion.60 = f32[1056,1024]{1,0:T(8,128)} fusion(f32[1056,1024]{1,0:T(8,128)} %get-tuple-element.17, f32[1024]{0:T(1024)S(1)} %bitcast.20, f32[1056]{0:T(1024)S(1)} %add_rsqrt_fusion.1, pred[1056]{0:T(1024)(128)(4,1)S(1)} %compare_and_fusion.1), kind=kLoop, calls=%fused_computation.116 | loop fusion | flops 5406720 | bytes 8660128 | tf_op jit(solution)/shard_map/convert_element_type | solution.py:27
  114.8 0.0 all-gather.9.cloned.1.call-done
  114.8 41.7 %multiply_reduce_fusion.2 = (f32[1040]{0:T(1024)S(1)}, f32[1040,1024]{1,0:T(8,128)}) fusion(f32[1024]{0:T(1024)S(1)} %bitcast.23, bf16[1,1,1024,1024]{3,2,1,0:T(8,128)(2,1)} %all-gather.9.cloned.1.call-done, f32[1056,1024]{1,0:T(8,128)} %fusion.60, f32[1040]{0:T(1024)S(1)} %maximum_convert_fusion.1, f32[]{:T(128)S(6)} %mul.631, f32[]{:T(128)S(6)} %mul.628, ...), kind=kOutput, calls=%fused_computation.75 | convolution fusion | flops 2223635456 | bytes 78786752 | tf_op jit(solution)/shard_map/tgc,gcd->tgd/dot_general | solution.py:70
  156.4 6.7 %psum.23 = f32[1040]{0:T(1024)S(1)} all-reduce(f32[1040]{0:T(1024)S(1)} %get-tuple-element.18), channel_id=1, replica_groups=mesh['sp'=8,'tp'=4] {'tp'}, use_global_device_ids=true, to_apply=%region_5.6 | all-reduce | flops 1040 | bytes 8320 | tf_op jit(solution)/shard_map/psum | solution.py:59
  163.1 4.7 %fusion.63 = f32[1040,1024]{1,0:T(8,128)} fusion(f32[1040,1024]{1,0:T(8,128)} %get-tuple-element.19, f32[1024]{0:T(1024)S(1)} %bitcast.19, f32[1040]{0:T(1024)S(1)} %add_rsqrt_fusion, pred[1040]{0:T(1024)(128)(4,1)S(1)} %compare_and_fusion), kind=kLoop, calls=%fused_computation.118 | loop fusion | flops 5324800 | bytes 8528976 | tf_op jit(solution)/shard_map/convert_element_type | solution.py:27
  167.8 0.0 all-gather.11.cloned.1.call-done
  167.8 39.2 %fusion.55 = bf16[1024,1024]{1,0:T(8,128)(2,1)} fusion(f32[1040,1024]{1,0:T(8,128)} %get-tuple-element.19, bf16[1,1,1024,1024]{3,2,1,0:T(8,128)(2,1)} %all-gather.11.cloned.1.call-done, f32[1024]{0:T(1024)S(1)} %bitcast.22, f32[1040,1024]{1,0:T(8,128)} %fusion.63, f32[1024]{0:T(1024)S(1)} %maximum_convert_fusion.3, f32[]{:T(128)S(6)} %mul.631, ...), kind=kOutput, calls=%fused_computation.110 | convolution fusion | flops 2186280960 | bytes 75505728 | tf_op jit(solution)/shard_map/tgc,gcd->tgd/dot_general | solution.py:70
  (9 shorter events, 0.1 us)
Async XLA Ops:
  6.5 14.7 %copy-start = (bf16[1024,1024]{1,0:T(8,128)(2,1)S(1)}, bf16[1024,1024]{1,0:T(8,128)(2,1)}, u32[]{:S(2)}) copy-start(bf16[1024,1024]{1,0:T(8,128)(2,1)} %param.4) | copy-start | bytes 6291460
  6.5 54.9 %all-gather.7.cloned.1.call-start = ((), (), s32[]{:S(2)}) async-start(), calls=%async_computation | async-start | bytes 2359296 | tf_op jit(solution)/shard_map/all_gather | solution.py:73
  8.7 106.1 %all-gather.9.cloned.1.call-start = ((), (), s32[]{:S(2)}) async-start(), calls=%async_computation.1 | async-start | bytes 2359296 | tf_op jit(solution)/shard_map/all_gather | solution.py:73
  9.5 158.3 %all-gather.11.cloned.1.call-start = ((), (), s32[]{:S(2)}) async-start(), calls=%async_computation.2 | async-start | bytes 2359296 | tf_op jit(solution)/shard_map/all_gather | solution.py:73
  10.4 8.3 %collective-permute-start = (bf16[24,1024]{1,0:T(8,128)(2,1)S(1)}, bf16[24,1024]{1,0:T(8,128)(2,1)S(1)}, u32[]{:S(2)}, u32[]{:S(2)}) collective-permute-start(bf16[24,1024]{1,0:T(8,128)(2,1)S(1)} %get-tuple-element.5), channel_id=1, source_target_pairs={{0,4},{4,8},{8,12},{12,16},{16,20},{20,24},{24,28},{1,5},{5,9},{9,... | collective-permute-start | bytes 147464 | tf_op jit(solution)/shard_map/ppermute | solution.py:20
  15.3 6.0 %collective-permute-start.1 = (bf16[24,1024]{1,0:T(8,128)(2,1)S(1)}, bf16[24,1024]{1,0:T(8,128)(2,1)S(1)}, u32[]{:S(2)}, u32[]{:S(2)}) collective-permute-start(bf16[24,1024]{1,0:T(8,128)(2,1)S(1)} %get-tuple-element.6), channel_id=1, source_target_pairs={{4,0},{8,4},{12,8},{16,12},{20,16},{24,20},{28,24},{5,1},{9,5},{13... | collective-permute-start | bytes 147464 | tf_op jit(solution)/shard_map/ppermute | solution.py:21
Sparse Core Ops, SparseCore 0:
  9.5 51.8 all-gather.6
  63.5 47.6 all-gather.8
  113.3 47.6 all-gather.10
where the time goes:
time: 214 us
  matrix products  123 us (57%)
  waiting for transfers between devices  31.3 us (15%)
  blocking collectives  19.2 us (9%)
  other arithmetic  17.3 us (8%)
  between operations  13.4 us (6%)
  starting transfers between devices  6.26 us (3%)
  local copies, waits for them, and re-layouts  3 us (1%)
    dot_general x3, matrix products, local(): jnp.einsum('tgc,gcd->tgd', pooled, lax.all_gather(pool_weight[layer_idx],...  123 us
    all_gather x3, waiting for transfers between devices, local(): lax.all_gather(pool_weight[layer_idx], 'sp', axis=1, tiled=True)  28 us
    psum x3, blocking collectives, local(): square_sums = lax.psum(jnp.sum(current_f * current_f, axis=1), 'tp')  19.2 us
    convert_element_type x3, other arithmetic, window_pool(): extended.astype(jnp.float32)  12.3 us
    ppermute x1, starting transfers between devices, padded(): before = lax.ppermute(last, axis, up)  4.89 us
  transfers between devices with their start and end apart: 5, of which 2 were waited for; matrix products, arithmetic and copies ran while one was open for 48% of the time, Pallas kernels for 0%

commit v1 on v0

v1 whole, which is shorter than its diff:
```python
import functools

import jax
import jax.numpy as jnp
from jax import lax
from jax.experimental import pallas as pl
from jax.experimental.pallas import tpu as pltpu
from jax.sharding import PartitionSpec as P

D = 4096
POOL_GROUPS = 4
NORM_EPS = 1e-06
PAD = 64
HALO = 32
TILE = 128
DOWN, UP, ACROSS = 0, 1, 2
MESH = pl.DeviceIdType.MESH


def unit_list(layers, width):
    eighth = width // 8
    units = []
    for layer in range(layers):
        along = 2 * eighth if layer == 0 else eighth
        cuts = [4 * eighth, width - along]
        if layer == layers - 1:
            cuts = [4 * eighth, 6 * eighth, width - along]
        units.append((layer, width - along, along, True))
        first = 0
        for cut in cuts:
            units.append((layer, first, cut - first, False))
            first = cut
    return units


def kernel(cfg, x_hbm, w_hbm, gain_ref, scale_ref, o_hbm, xs, ns, ps, ws, ss_own, ss_in,
           load_sem, halo_send, halo_recv, ss_send, ss_recv, w_send, w_recv, out_sem):
    layers, rows, width, shard_rows, n_sp, n_tp, in_kernel = cfg
    sp, tp = lax.axis_index("sp"), lax.axis_index("tp")
    line = n_sp // 2
    z, y = sp // 2, sp % 2
    units = unit_list(layers, width)
    total_rows = rows + 2 * PAD
    tiles = total_rows // TILE
    seq_total = rows * n_sp
    base_pos = sp * rows - PAD
    half = jnp.left_shift(jnp.int32(1), tp)

    has_down, has_up = z > 0, z < line - 1
    has_prev, has_next = sp > 0, sp < n_sp - 1
    target = {DOWN: (sp - 2, tp), UP: (sp + 2, tp), ACROSS: (z * 2 + (1 - y), tp)}

    x_load = pltpu.make_async_copy(x_hbm, xs.at[pl.ds(PAD, rows)], load_sem.at[layers])
    own_rows = pl.ds(pl.multiple_of(sp * shard_rows, shard_rows), shard_rows)
    if in_kernel:
        w_loads = [
            pltpu.make_async_copy(w_hbm.at[l, 0], ws.at[l, own_rows], load_sem.at[l])
            for l in range(layers)
        ]
    else:
        w_loads = [
            pltpu.make_async_copy(w_hbm.at[l, 0], ws.at[l], load_sem.at[l])
            for l in range(layers)
        ]
    w_loads[0].start()
    x_load.start()
    for l in range(1, layers):
        w_loads[l].start()

    barrier = pltpu.get_barrier_semaphore()

    def greet(device):
        pl.semaphore_signal(barrier, inc=1, device_id=device, device_id_type=MESH)

    expected = jnp.int32(n_tp - 1)
    for p in range(1, n_tp):
        greet((sp, lax.rem(tp + p, n_tp)))
    pl.when(has_prev)(lambda: greet((sp - 1, tp)))
    pl.when(has_next)(lambda: greet((sp + 1, tp)))
    expected = expected + has_prev.astype(jnp.int32) + has_next.astype(jnp.int32)
    if in_kernel:
        greet(target[ACROSS])
        pl.when(has_down)(lambda: greet(target[DOWN]))
        pl.when(has_up)(lambda: greet(target[UP]))
        expected = expected + 1 + has_down.astype(jnp.int32) + has_up.astype(jnp.int32)

    zero = jnp.zeros((PAD, width), jnp.bfloat16)
    ns[pl.ds(0, PAD)] = zero
    ns[pl.ds(total_rows + PAD, PAD)] = zero
    xs[pl.ds(0, PAD - HALO)] = zero[: PAD - HALO]
    xs[pl.ds(PAD + rows + HALO, PAD - HALO)] = zero[: PAD - HALO]

    @pl.when(jnp.logical_not(has_prev))
    def _():
        xs[pl.ds(PAD - HALO, HALO)] = zero[:HALO]

    @pl.when(jnp.logical_not(has_next))
    def _():
        xs[pl.ds(PAD + rows, HALO)] = zero[:HALO]

    pl.semaphore_wait(barrier, expected)

    to_next = pltpu.make_async_remote_copy(
        x_hbm.at[pl.ds(rows - HALO, HALO)], xs.at[pl.ds(PAD - HALO, HALO)],
        halo_send.at[0], halo_recv.at[0], device_id=(sp + 1, tp), device_id_type=MESH)
    to_prev = pltpu.make_async_remote_copy(
        x_hbm.at[pl.ds(0, HALO)], xs.at[pl.ds(PAD + rows, HALO)],
        halo_send.at[1], halo_recv.at[1], device_id=(sp - 1, tp), device_id_type=MESH)
    pl.when(has_next)(lambda: to_next.start())
    pl.when(has_prev)(lambda: to_prev.start())

    def piece(u, j, col):
        layer, first, columns, _ = units[u]
        start = pl.multiple_of((j * 2 + col) * shard_rows, shard_rows)
        return ws.at[layer, pl.ds(start, shard_rows), pl.ds(first, columns)]

    def copy(way, u, j, col):
        at = j * 2 + col
        return pltpu.make_async_remote_copy(
            piece(u, j, col), piece(u, j, col), w_send.at[way, u, at], w_recv.at[u, at],
            device_id=target[way], device_id_type=MESH)

    def arrive(u, j, col):
        copy(ACROSS, u, j, col).wait_recv()

    def send_own(u):
        pl.when(has_down)(lambda: copy(DOWN, u, z, y).start())
        pl.when(has_up)(lambda: copy(UP, u, z, y).start())
        copy(ACROSS, u, z, y).start()

    def pass_own_row(u):
        arrive(u, z, 1 - y)
        pl.when(has_down)(lambda: copy(DOWN, u, z, 1 - y).start())
        pl.when(has_up)(lambda: copy(UP, u, z, 1 - y).start())

    def forward(u, step):
        along = units[u][3]

        def hop(j, way, more):
            arrive(u, j, y)
            pl.when(more)(lambda: copy(way, u, j, y).start())
            if along:
                arrive(u, j, 1 - y)
                pl.when(more)(lambda: copy(way, u, j, 1 - y).start())
            else:
                copy(ACROSS, u, j, y).start()

        pl.when(z + step < line)(lambda: hop(z + step, DOWN, has_down))
        pl.when(z - step >= 0)(lambda: hop(z - step, UP, has_up))

    def arrive_across(u):
        if not units[u][3]:
            for j in range(line):
                arrive(u, j, 1 - y)

    def tile_rows(i):
        return pl.ds(pl.multiple_of(i * TILE, TILE), TILE)

    def square_sums(layer):
        @pl.loop(0, tiles)
        def _(i):
            part = jnp.zeros((TILE, 128), jnp.float32)
            for c in range(width // 128):
                v = xs[tile_rows(i), pl.ds(c * 128, 128)].astype(jnp.float32)
                part = part + v * v
            ss_own[layer, pl.ds(i, 1)] = jnp.sum(part.T, axis=0, keepdims=True)

    def ss_copy(layer, p):
        return pltpu.make_async_remote_copy(
            ss_own.at[layer], ss_in.at[layer, p - 1], ss_send.at[layer, p - 1], ss_recv.at[layer, p - 1],
            device_id=(sp, lax.rem(tp + p, n_tp)), device_id_type=MESH)

    def send_sums(layer):
        square_sums(layer)
        for p in range(1, n_tp):
            ss_copy(layer, p).start()

    def wait_sums(layer):
        for p in range(1, n_tp):
            ss_copy(layer, p).wait()

    def normalise(layer, lo, hi):
        @pl.loop(lo, hi)
        def _(i):
            total = ss_own[layer, pl.ds(i, 1)]
            for p in range(1, n_tp):
                total = total + ss_in[layer, p - 1, pl.ds(i, 1)]
            factor = lax.rsqrt(total / D + NORM_EPS)
            pos = base_pos + i * TILE + lax.broadcasted_iota(jnp.int32, (1, TILE), 1)
            factor = jnp.where((pos >= 0) & (pos < seq_total), factor, 0.0)
            column = jnp.broadcast_to(factor, (TILE, TILE)).T
            for c in range(width // 128):
                cols = pl.ds(c * 128, 128)
                v = xs[tile_rows(i), cols].astype(jnp.float32)
                g = gain_ref[layer : layer + 1, cols].astype(jnp.float32)
                ns[pl.ds(pl.multiple_of(PAD + i * TILE, 64), TILE), cols] = (v * column * g).astype(jnp.bfloat16)

    window = TILE + 2 * PAD

    def pool(lo, hi):
        @pl.loop(lo, hi)
        def _(i):
            offset = (
                lax.broadcasted_iota(jnp.int32, (TILE, window), 1)
                - lax.broadcasted_iota(jnp.int32, (TILE, window), 0)
                - PAD
            )
            pos = base_pos + i * TILE + lax.broadcasted_iota(jnp.int32, (TILE, window), 0)
            count = jnp.minimum(pos + half, seq_total) - jnp.maximum(pos - half, 0)
            count = jnp.maximum(count, 1).astype(jnp.float32)
            band = jnp.where((offset >= -half) & (offset < half), 1.0, 0.0)
            band = (band - jnp.where(offset == 0, count, 0.0)).astype(jnp.bfloat16)
            inverse = 1.0 / count[:, :1]
            rows_in = pl.ds(pl.multiple_of(i * TILE, TILE), window)
            for c in range(width // 256):
                cols = pl.ds(c * 256, 256)
                sums = jnp.dot(band, ns[rows_in, cols], preferred_element_type=jnp.float32)
                ps[tile_rows(i), cols] = (sums * inverse).astype(jnp.bfloat16)

    def mix(layer, first_row, block, first, columns):
        cols = pl.ds(first, columns)
        at = pl.ds(pl.multiple_of(first_row, 64), block)
        branch = jnp.dot(ps[at], ws[layer, :, cols], preferred_element_type=jnp.float32)
        s = scale_ref[layer : layer + 1, cols].astype(jnp.float32)
        xs[at, cols] = (xs[at, cols].astype(jnp.float32) + branch * s).astype(jnp.bfloat16)

    third = tiles // 3
    thirds = [(0, third), (third, 2 * third), (2 * third, tiles)]

    def mix_block(layer, lo, hi):
        def run():
            for c in range(width // 256):
                mix(layer, lo * TILE, (hi - lo) * TILE, c * 256, 256)
        return run

    def prepare(layer):
        work = [lambda: send_sums(layer), lambda: None]
        first = [True]

        def norm(lo, hi):
            if first[0]:
                wait_sums(layer)
                first[0] = False
            normalise(layer, lo, hi)

        work += [functools.partial(norm, lo, hi) for lo, hi in thirds]
        work += [functools.partial(pool, lo, hi) for lo, hi in thirds]
        return work

    def start_work():
        x_load.wait()
        pl.when(has_prev)(lambda: to_next.wait_recv())
        pl.when(has_next)(lambda: to_prev.wait_recv())

    if in_kernel:
        count = len(units)
        w_loads[0].wait()
        waited = 0
        for u in range(2):
            send_own(u)
        ahead = 2
        tasks = [start_work] + prepare(0)
        for u in range(count):
            layer, along = units[u][0], units[u][3]
            if ahead < count:
                if units[ahead][0] > waited:
                    waited = units[ahead][0]
                    w_loads[waited].wait()
                send_own(ahead)
                ahead += 1
            if along:
                pass_own_row(u)
            for step in range(1, line):
                forward(u, step)
                if tasks:
                    tasks.pop(0)()
            if along and layer > 0:
                while tasks:
                    tasks.pop(0)()
                for v in range(count):
                    if units[v][0] == layer - 1:
                        arrive_across(v)
                tasks = [mix_block(layer - 1, lo, hi) for lo, hi in thirds] + prepare(layer)
        while tasks:
            tasks.pop(0)()
    else:
        start_work()
        for layer in range(layers):
            for task in prepare(layer):
                task()
            w_loads[layer].wait()
            if layer < layers - 1:
                for lo, hi in thirds:
                    mix_block(layer, lo, hi)()

    outs = []
    for u, (layer, first, columns, _) in enumerate(units):
        if layer < layers - 1:
            continue
        if in_kernel:
            arrive_across(u)

        @pl.loop(0, rows // 256)
        def _(i):
            mix(layer, PAD + i * 256, 256, first, columns)

        out = pltpu.make_async_copy(
            xs.at[pl.ds(PAD, rows), pl.ds(first, columns)], o_hbm.at[:, pl.ds(first, columns)], out_sem.at[len(outs)])
        out.start()
        outs.append(out)

    pl.when(has_next)(lambda: to_next.wait_send())
    pl.when(has_prev)(lambda: to_prev.wait_send())
    if in_kernel:
        for u in range(len(units)):
            along = units[u][3]
            for j in range(line):
                def done(way, col):
                    copy(way, u, j, col).wait_send()

                @pl.when(has_down & (j >= z))
                def _():
                    done(DOWN, y)
                    if along:
                        done(DOWN, 1 - y)

                @pl.when(has_up & (j <= z))
                def _():
                    done(UP, y)
                    if along:
                        done(UP, 1 - y)

                if along:
                    pl.when(z == j)(lambda: done(ACROSS, y))
                else:
                    done(ACROSS, y)
    for out in outs:
        out.wait()


def solution(mesh):
    n_sp, n_tp = mesh.shape["sp"], mesh.shape["tp"]
    in_kernel = n_sp % 2 == 0 and n_sp <= 16

    def local(stream, norm_gain, pool_weight, pool_scale):
        rows, _ = stream.shape
        layers, per_dev, shard_rows, width = pool_weight.shape
        assert per_dev == 1 and n_tp == POOL_GROUPS
        if not in_kernel:
            pool_weight = lax.all_gather(pool_weight, "sp", axis=2, tiled=True)
        total_rows = rows + 2 * PAD
        units = len(unit_list(layers, width)) if in_kernel else 1
        dma = pltpu.SemaphoreType.DMA
        any_space = pl.BlockSpec(memory_space=pl.ANY)
        vmem = pl.BlockSpec(memory_space=pltpu.VMEM)
        return pl.pallas_call(
            functools.partial(kernel, (layers, rows, width, shard_rows, n_sp, n_tp, in_kernel)),
            out_shape=jax.ShapeDtypeStruct((rows, width), jnp.bfloat16),
            in_specs=[any_space, any_space, vmem, vmem],
            out_specs=any_space,
            scratch_shapes=[
                pltpu.VMEM((total_rows, width), jnp.bfloat16),
                pltpu.VMEM((total_rows + 2 * PAD, width), jnp.bfloat16),
                pltpu.VMEM((total_rows, width), jnp.bfloat16),
                pltpu.VMEM((layers, width, width), jnp.bfloat16),
                pltpu.VMEM((layers, 16, TILE), jnp.float32),
                pltpu.VMEM((layers, n_tp - 1, 16, TILE), jnp.float32),
                dma((layers + 1,)),
                dma((2,)),
                dma((2,)),
                dma((layers, n_tp - 1)),
                dma((layers, n_tp - 1)),
                dma((3, units, n_sp)),
                dma((units, n_sp)),
                dma((4,)),
            ],
            compiler_params=pltpu.CompilerParams(
                collective_id=0, has_side_effects=True, vmem_limit_bytes=60 * 2**20
            ),
        )(stream, pool_weight, norm_gain, pool_scale)

    placed = (P("sp", "tp"), P(None, "tp"), P(None, "tp", "sp", None), P(None, "tp"))
    return jax.shard_map(
        local, mesh=mesh, in_specs=placed, out_specs=P("sp", "tp"), check_vma=False
    )
```

time: 214 us -> 99.8 us (0.47)
  matrix products: 123 us -> 0 us
  Pallas kernels: 0 us -> 96.5 us
  waiting for transfers between devices: 31.3 us -> 0 us
  blocking collectives: 19.2 us -> 0 us
  other arithmetic: 17.3 us -> 0 us
  between operations: 13.4 us -> 0.01 us
  starting transfers between devices: 6.26 us -> 0 us
    dot_general x3 -> x0, matrix products: 123 us -> none  [local(): jnp.einsum('tgc,gcd->tgd', pooled, lax.all_gather(pool_weight[layer_idx],...]
    pallas_call x0 -> x1, Pallas kernels: none -> 96.5 us  [local(): pl.pallas_call(functools.partial(kernel, (layers, rows, width, shard_rows...]
    all_gather x3 -> x0, waiting for transfers between devices: 28 us -> none  [local(): lax.all_gather(pool_weight[layer_idx], 'sp', axis=1, tiled=True)]
    psum x3 -> x0, blocking collectives: 19.2 us -> none  [local(): square_sums = lax.psum(jnp.sum(current_f * current_f, axis=1), 'tp')]
    convert_element_type x7 -> x0, other arithmetic: 15.1 us -> none  [the longest x3 12.3 us: window_pool(): extended.astype(jnp.float32)]
    ppermute x2 -> x0, starting transfers between devices: 6.18 us -> none  [the longest x1 4.89 us: padded(): before = lax.ppermute(last, axis, up)]
    unnamed x2 -> x1, local copies, waits for them, and re-layouts: 0.01 us -> 3.08 us
    slice x2 -> x0, local copies, waits for them, and re-layouts: 3 us -> none  [the longest x1 2.16 us: local(): pool_weight[layer_idx]]
  transfers between devices with their start and end apart: 5 -> 0, of which waited for: 2 -> 0; matrix products, arithmetic and copies ran while one was open for 48% -> 0% of each run, Pallas kernels for 0% -> 0%
where the time goes in v1:
time: 99.8 us; the launch traced here: 99.6 us
  Pallas kernels  96.5 us (97%)
  local copies, waits for them, and re-layouts  3.08 us (3%)
    pallas_call x1, Pallas kernels, local(): pl.pallas_call(functools.partial(kernel, (layers, rows, width, shard_rows...  96.5 us
    unnamed x1, local copies, waits for them, and re-layouts  3.08 us

profile of v1, /device:TPU:0, one launch (start us, length us, event | category | flops | bytes accessed | tf_op | source)
XLA Modules:
  0.0 99.6 jit_solution(34064507719739165)
XLA Ops:
  0.0 96.5 %shard_map.46 = bf16[1024,1024]{1,0:T(8,128)(2,1)} custom-call(bf16[1024,1024]{1,0:T(8,128)(2,1)} %x_hbm.1, bf16[3,1,128,1024]{3,2,1,0:T(8,128)(2,1)} %w_hbm.1, bf16[3,1024]{1,0:T(4,128)(2,1)} %gain_ref.1, bf16[3,1024]{1,0:T(4,128)(2,1)} %scale_ref.1), custom_call_target="tpu_custom_call" | custom-call | tf_op jit(solution)/shard_map/pallas_call | solution.py:356
  96.5 3.1 %copy.6 = bf16[1024,1024]{1,0:T(8,128)(2,1)} copy(bf16[1024,1024]{1,0:T(8,128)(2,1)} %shard_map.46) | data formatting | bytes 4194304

commit v2 on v1

--- a/solution.py
+++ b/solution.py
@@ -17,24 +17,25 @@
 MESH = pl.DeviceIdType.MESH
 
 
+LEAD, SKEW, EARLY = 5, 3, 2
+MIX_AT = 6
+
+
 def unit_list(layers, width):
     eighth = width // 8
     units = []
     for layer in range(layers):
-        along = 2 * eighth if layer == 0 else eighth
-        cuts = [4 * eighth, width - along]
-        if layer == layers - 1:
-            cuts = [4 * eighth, 6 * eighth, width - along]
-        units.append((layer, width - along, along, True))
+        sizes = [3, 2, 2] if layer == layers - 1 else [2, 2, 3]
+        units.append((layer, 7 * eighth, eighth, True))
         first = 0
-        for cut in cuts:
-            units.append((layer, first, cut - first, False))
-            first = cut
+        for size in sizes:
+            units.append((layer, first * eighth, size * eighth, False))
+            first += size
     return units
 
 
-def kernel(cfg, x_hbm, w_hbm, gain_ref, scale_ref, o_hbm, xs, ns, ps, ws, ss_own, ss_in,
-           load_sem, halo_send, halo_recv, ss_send, ss_recv, w_send, w_recv, out_sem):
+def kernel(cfg, x_hbm, w_hbm, gain_ref, scale_ref, out_ref, xs, ns, ps, ws, ss_own, ss_in,
+           load_sem, halo_send, halo_recv, ss_send, ss_recv, w_send, w_recv):
     layers, rows, width, shard_rows, n_sp, n_tp, in_kernel = cfg
     sp, tp = lax.axis_index("sp"), lax.axis_index("tp")
     line = n_sp // 2
@@ -217,12 +218,16 @@
                 sums = jnp.dot(band, ns[rows_in, cols], preferred_element_type=jnp.float32)
                 ps[tile_rows(i), cols] = (sums * inverse).astype(jnp.bfloat16)
 
-    def mix(layer, first_row, block, first, columns):
+    def mix(layer, first_row, block, first, columns, out=False):
         cols = pl.ds(first, columns)
         at = pl.ds(pl.multiple_of(first_row, 64), block)
         branch = jnp.dot(ps[at], ws[layer, :, cols], preferred_element_type=jnp.float32)
         s = scale_ref[layer : layer + 1, cols].astype(jnp.float32)
-        xs[at, cols] = (xs[at, cols].astype(jnp.float32) + branch * s).astype(jnp.bfloat16)
+        mixed = (xs[at, cols].astype(jnp.float32) + branch * s).astype(jnp.bfloat16)
+        if out:
+            out_ref[pl.ds(pl.multiple_of(first_row - PAD, 64), block), cols] = mixed
+        else:
+            xs[at, cols] = mixed
 
     third = tiles // 3
     thirds = [(0, third), (third, 2 * third), (2 * third, tiles)]
@@ -253,34 +258,40 @@
         pl.when(has_next)(lambda: to_prev.wait_recv())
 
     if in_kernel:
-        count = len(units)
         w_loads[0].wait()
-        waited = 0
-        for u in range(2):
+        loaded = [0]
+
+        def own(u):
+            if units[u][0] > loaded[0]:
+                loaded[0] = units[u][0]
+                w_loads[loaded[0]].wait()
             send_own(u)
-        ahead = 2
+
         tasks = [start_work] + prepare(0)
-        for u in range(count):
-            layer, along = units[u][0], units[u][3]
-            if ahead < count:
-                if units[ahead][0] > waited:
-                    waited = units[ahead][0]
-                    w_loads[waited].wait()
-                send_own(ahead)
-                ahead += 1
-            if along:
-                pass_own_row(u)
+
+        def next_layer(layer):
+            while tasks:
+                tasks.pop(0)()
+            for v in range(len(units)):
+                if units[v][0] == layer - 1:
+                    arrive_across(v)
+            tasks.extend([mix_block(layer - 1, lo, hi) for lo, hi in thirds] + prepare(layer))
+
+        events = []
+        place = 0
+        for u in range(len(units)):
+            events.append((place - LEAD, 0, u, functools.partial(own, u)))
+            if units[u][3]:
+                events.append((place - EARLY, 1, u, functools.partial(pass_own_row, u)))
             for step in range(1, line):
-                forward(u, step)
-                if tasks:
-                    tasks.pop(0)()
-            if along and layer > 0:
-                while tasks:
-                    tasks.pop(0)()
-                for v in range(count):
-                    if units[v][0] == layer - 1:
-                        arrive_across(v)
-                tasks = [mix_block(layer - 1, lo, hi) for lo, hi in thirds] + prepare(layer)
+                events.append((place + SKEW * (step - 1), 2 + step, u, functools.partial(forward, u, step)))
+            place += units[u][2] // (width // 8)
+        for layer in range(1, layers):
+            events.append((8 * layer + MIX_AT, 2, 0, functools.partial(next_layer, layer)))
+        for _, kind, _, event in sorted(events, key=lambda e: e[:3]):
+            event()
+            if kind > 2 and tasks:
+                tasks.pop(0)()
         while tasks:
             tasks.pop(0)()
     else:
@@ -293,7 +304,6 @@
                 for lo, hi in thirds:
                     mix_block(layer, lo, hi)()
 
-    outs = []
     for u, (layer, first, columns, _) in enumerate(units):
         if layer < layers - 1:
             continue
@@ -302,12 +312,7 @@
 
         @pl.loop(0, rows // 256)
         def _(i):
-            mix(layer, PAD + i * 256, 256, first, columns)
-
-        out = pltpu.make_async_copy(
-            xs.at[pl.ds(PAD, rows), pl.ds(first, columns)], o_hbm.at[:, pl.ds(first, columns)], out_sem.at[len(outs)])
-        out.start()
-        outs.append(out)
+            mix(layer, PAD + i * 256, 256, first, columns, out=True)
 
     pl.when(has_next)(lambda: to_next.wait_send())
     pl.when(has_prev)(lambda: to_prev.wait_send())
@@ -334,8 +339,6 @@
                     pl.when(z == j)(lambda: done(ACROSS, y))
                 else:
                     done(ACROSS, y)
-    for out in outs:
-        out.wait()
 
 
 def solution(mesh):
@@ -351,13 +354,13 @@
         total_rows = rows + 2 * PAD
         units = len(unit_list(layers, width)) if in_kernel else 1
         dma = pltpu.SemaphoreType.DMA
-        any_space = pl.BlockSpec(memory_space=pl.ANY)
+        hbm = pl.BlockSpec(memory_space=pltpu.HBM)
         vmem = pl.BlockSpec(memory_space=pltpu.VMEM)
         return pl.pallas_call(
             functools.partial(kernel, (layers, rows, width, shard_rows, n_sp, n_tp, in_kernel)),
             out_shape=jax.ShapeDtypeStruct((rows, width), jnp.bfloat16),
-            in_specs=[any_space, any_space, vmem, vmem],
-            out_specs=any_space,
+            in_specs=[hbm, hbm, vmem, vmem],
+            out_specs=vmem,
             scratch_shapes=[
                 pltpu.VMEM((total_rows, width), jnp.bfloat16),
                 pltpu.VMEM((total_rows + 2 * PAD, width), jnp.bfloat16),
@@ -372,10 +375,9 @@
                 dma((layers, n_tp - 1)),
                 dma((3, units, n_sp)),
                 dma((units, n_sp)),
-                dma((4,)),
             ],
             compiler_params=pltpu.CompilerParams(
-                collective_id=0, has_side_effects=True, vmem_limit_bytes=60 * 2**20
+                collective_id=0, has_side_effects=True, vmem_limit_bytes=24 * 2**20
             ),
         )(stream, pool_weight, norm_gain, pool_scale)
 

time: 99.8 us -> 84.5 us (0.85)
  Pallas kernels: 96.5 us -> 78.7 us
  local copies, waits for them, and re-layouts: 3.08 us -> 5.44 us
    pallas_call x1, Pallas kernels: 96.5 us -> 78.7 us  [local(): pl.pallas_call(functools.partial(kernel, (layers, rows, width, shard_rows...]
    unnamed x1 -> x9, local copies, waits for them, and re-layouts: 3.08 us -> 5.44 us
where the time goes in v2:
time: 84.5 us; the launch traced here: 84.2 us
  Pallas kernels  78.7 us (93%)
  local copies, waits for them, and re-layouts  5.44 us (6%)
    pallas_call x1, Pallas kernels, local(): pl.pallas_call(functools.partial(kernel, (layers, rows, width, shard_rows...  78.7 us
    unnamed x9, local copies, waits for them, and re-layouts  5.44 us

profile of v2, /device:TPU:0, one launch (start us, length us, event | category | flops | bytes accessed | tf_op | source)
XLA Modules:
  0.0 84.2 jit_solution(12784420819650233185)
XLA Ops:
  0.0 0.0 copy-start
  0.0 1.6 %copy-done = bf16[1024,1024]{1,0:T(8,128)(2,1)S(1)} copy-done((bf16[1024,1024]{1,0:T(8,128)(2,1)S(1)}, bf16[1024,1024]{1,0:T(8,128)(2,1)}, u32[]{:S(2)}) %copy-start) | copy-done | bytes 2097176
  1.6 0.0 copy-start.1
  1.6 1.1 %copy-done.1 = bf16[3,1,128,1024]{3,2,1,0:T(8,128)(2,1)S(1)} copy-done((bf16[3,1,128,1024]{3,2,1,0:T(8,128)(2,1)S(1)}, bf16[3,1,128,1024]{3,2,1,0:T(8,128)(2,1)}, u32[]{:S(2)}) %copy-start.1) | copy-done | bytes 786456
  2.7 0.0 copy-start.2
  2.7 0.7 copy-done.2
  3.4 0.0 copy-start.3
  3.4 0.7 copy-done.3
  4.1 78.7 %shard_map.46 = bf16[1024,1024]{1,0:T(8,128)(2,1)S(1)} custom-call(bf16[1024,1024]{1,0:T(8,128)(2,1)S(1)} %copy-done, bf16[3,1,128,1024]{3,2,1,0:T(8,128)(2,1)S(1)} %copy-done.1, bf16[3,1024]{1,0:T(4,128)(2,1)S(1)} %copy-done.2, bf16[3,1024]{1,0:T(4,128)(2,1)S(1)} %copy-done.3), custom_call_target="tpu_custom_call" | custom-call | tf_op jit(solution)/shard_map/pallas_call | solution.py:359
  82.9 1.3 %copy.6 = bf16[1024,1024]{1,0:T(8,128)(2,1)} copy(bf16[1024,1024]{1,0:T(8,128)(2,1)S(1)} %shard_map.46) | data formatting | bytes 4194304
Async XLA Ops:
  0.0 1.6 %copy-start = (bf16[1024,1024]{1,0:T(8,128)(2,1)S(1)}, bf16[1024,1024]{1,0:T(8,128)(2,1)}, u32[]{:S(2)}) copy-start(bf16[1024,1024]{1,0:T(8,128)(2,1)} %x_hbm.1) | copy-start | bytes 6291460
  1.6 1.1 %copy-start.1 = (bf16[3,1,128,1024]{3,2,1,0:T(8,128)(2,1)S(1)}, bf16[3,1,128,1024]{3,2,1,0:T(8,128)(2,1)}, u32[]{:S(2)}) copy-start(bf16[3,1,128,1024]{3,2,1,0:T(8,128)(2,1)} %w_hbm.1) | copy-start | bytes 2359300
  2.7 0.7 copy-start.2
  3.4 0.7 copy-start.3

commit v3 on v2

--- a/solution.py
+++ b/solution.py
@@ -34,8 +34,8 @@
     return units
 
 
-def kernel(cfg, x_hbm, w_hbm, gain_ref, scale_ref, out_ref, xs, ns, ps, ws, ss_own, ss_in,
-           load_sem, halo_send, halo_recv, ss_send, ss_recv, w_send, w_recv):
+def kernel(cfg, x_hbm, w_hbm, gain_hbm, scale_hbm, out_ref, gain_ref, scale_ref, xs, ns, ps, ws, ss_own, ss_in,
+           load_sem, halo_send, halo_recv, ss_send, ss_recv, w_send, w_recv, out_sem):
     layers, rows, width, shard_rows, n_sp, n_tp, in_kernel = cfg
     sp, tp = lax.axis_index("sp"), lax.axis_index("tp")
     line = n_sp // 2
@@ -65,6 +65,10 @@
         ]
     w_loads[0].start()
     x_load.start()
+    gain_load = pltpu.make_async_copy(gain_hbm, gain_ref, load_sem.at[layers + 1])
+    scale_load = pltpu.make_async_copy(scale_hbm, scale_ref, load_sem.at[layers + 2])
+    gain_load.start()
+    scale_load.start()
     for l in range(1, layers):
         w_loads[l].start()
 
@@ -218,16 +222,13 @@
                 sums = jnp.dot(band, ns[rows_in, cols], preferred_element_type=jnp.float32)
                 ps[tile_rows(i), cols] = (sums * inverse).astype(jnp.bfloat16)
 
-    def mix(layer, first_row, block, first, columns, out=False):
+    def mix(layer, first_row, block, first, columns):
         cols = pl.ds(first, columns)
         at = pl.ds(pl.multiple_of(first_row, 64), block)
         branch = jnp.dot(ps[at], ws[layer, :, cols], preferred_element_type=jnp.float32)
         s = scale_ref[layer : layer + 1, cols].astype(jnp.float32)
         mixed = (xs[at, cols].astype(jnp.float32) + branch * s).astype(jnp.bfloat16)
-        if out:
-            out_ref[pl.ds(pl.multiple_of(first_row - PAD, 64), block), cols] = mixed
-        else:
-            xs[at, cols] = mixed
+        xs[at, cols] = mixed
 
     third = tiles // 3
     thirds = [(0, third), (third, 2 * third), (2 * third, tiles)]
@@ -254,6 +255,8 @@
 
     def start_work():
         x_load.wait()
+        gain_load.wait()
+        scale_load.wait()
         pl.when(has_prev)(lambda: to_next.wait_recv())
         pl.when(has_next)(lambda: to_prev.wait_recv())
 
@@ -304,6 +307,7 @@
                 for lo, hi in thirds:
                     mix_block(layer, lo, hi)()
 
+    outs = []
     for u, (layer, first, columns, _) in enumerate(units):
         if layer < layers - 1:
             continue
@@ -312,7 +316,11 @@
 
         @pl.loop(0, rows // 256)
         def _(i):
-            mix(layer, PAD + i * 256, 256, first, columns, out=True)
+            mix(layer, PAD + i * 256, 256, first, columns)
+
+        outs.append(pltpu.make_async_copy(
+            xs.at[pl.ds(PAD, rows), pl.ds(first, columns)], out_ref.at[:, pl.ds(first, columns)], out_sem.at[len(outs)]))
+        outs[-1].start()
 
     pl.when(has_next)(lambda: to_next.wait_send())
     pl.when(has_prev)(lambda: to_prev.wait_send())
@@ -339,6 +347,8 @@
                     pl.when(z == j)(lambda: done(ACROSS, y))
                 else:
                     done(ACROSS, y)
+    for out in outs:
+        out.wait()
 
 
 def solution(mesh):
@@ -355,29 +365,31 @@
         units = len(unit_list(layers, width)) if in_kernel else 1
         dma = pltpu.SemaphoreType.DMA
         hbm = pl.BlockSpec(memory_space=pltpu.HBM)
-        vmem = pl.BlockSpec(memory_space=pltpu.VMEM)
         return pl.pallas_call(
             functools.partial(kernel, (layers, rows, width, shard_rows, n_sp, n_tp, in_kernel)),
             out_shape=jax.ShapeDtypeStruct((rows, width), jnp.bfloat16),
-            in_specs=[hbm, hbm, vmem, vmem],
-            out_specs=vmem,
+            in_specs=[hbm] * 4,
+            out_specs=hbm,
             scratch_shapes=[
+                pltpu.VMEM((layers, width), jnp.bfloat16),
+                pltpu.VMEM((layers, width), jnp.bfloat16),
                 pltpu.VMEM((total_rows, width), jnp.bfloat16),
                 pltpu.VMEM((total_rows + 2 * PAD, width), jnp.bfloat16),
                 pltpu.VMEM((total_rows, width), jnp.bfloat16),
                 pltpu.VMEM((layers, width, width), jnp.bfloat16),
                 pltpu.VMEM((layers, 16, TILE), jnp.float32),
                 pltpu.VMEM((layers, n_tp - 1, 16, TILE), jnp.float32),
-                dma((layers + 1,)),
+                dma((layers + 3,)),
                 dma((2,)),
                 dma((2,)),
                 dma((layers, n_tp - 1)),
                 dma((layers, n_tp - 1)),
                 dma((3, units, n_sp)),
                 dma((units, n_sp)),
+                dma((4,)),
             ],
             compiler_params=pltpu.CompilerParams(
-                collective_id=0, has_side_effects=True, vmem_limit_bytes=24 * 2**20
+                collective_id=0, has_side_effects=True, vmem_limit_bytes=60 * 2**20
             ),
         )(stream, pool_weight, norm_gain, pool_scale)
 

time: 84.5 us -> 82.7 us (0.979)
  local copies, waits for them, and re-layouts: 5.44 us -> 3.08 us
    unnamed x9 -> x1, local copies, waits for them, and re-layouts: 5.44 us -> 3.08 us
where the time goes in v3:
time: 82.7 us; the launch traced here: 82.6 us
  Pallas kernels  79.5 us (96%)
  local copies, waits for them, and re-layouts  3.08 us (4%)
    pallas_call x1, Pallas kernels, local(): pl.pallas_call(functools.partial(kernel, (layers, rows, width, shard_rows...  79.5 us
    unnamed x1, local copies, waits for them, and re-layouts  3.08 us

profile of v3, /device:TPU:0, one launch (start us, length us, event | category | flops | bytes accessed | tf_op | source)
XLA Modules:
  0.0 82.6 jit_solution(8350618627425019270)
XLA Ops:
  0.0 79.5 %shard_map.46 = bf16[1024,1024]{1,0:T(8,128)(2,1)} custom-call(bf16[1024,1024]{1,0:T(8,128)(2,1)} %x_hbm.1, bf16[3,1,128,1024]{3,2,1,0:T(8,128)(2,1)} %w_hbm.1, bf16[3,1024]{1,0:T(4,128)(2,1)} %gain_hbm.1, bf16[3,1024]{1,0:T(4,128)(2,1)} %scale_hbm.1), custom_call_target="tpu_custom_call" | custom-call | tf_op jit(solution)/shard_map/pallas_call | solution.py:368
  79.5 3.1 %copy.6 = bf16[1024,1024]{1,0:T(8,128)(2,1)} copy(bf16[1024,1024]{1,0:T(8,128)(2,1)} %shard_map.46) | data formatting | bytes 4194304
